TPU v7x, 32 devices: a whole 2x2x4 slice. The times are simulated.
32 devices in a mesh: grp: 2 (over y), ep: 4 (over z), tp: 4 (over x, core).
Axes of the slice: x: 2, y: 2, z: 4, core: 2. Of those that a mesh axis runs over, the one named last changes fastest.
Arguments:
- out_gate: bfloat16 [1536, 4096], P(('grp', 'ep'), 'tp'), parts along dimension 0, may hold values from -6 to 6
- in_gate: bfloat16 [1536, 4096], P(('grp', 'ep'), 'tp'), parts along dimension 0, may hold values from -6 to 6
- values: bfloat16 [1536, 4096], P(('grp', 'ep'), 'tp'), parts along dimension 0, may hold values from -6 to 6
- conv_taps: float32 [3, 4096], P(None, 'tp'), may hold values from -3 to 3
- mixer_weight: bfloat16 [4096, 4096], P(None, 'tp'), may hold values from -0.09375 to 0.09375
- expert_input: bfloat16 [1536, 4096], P(('grp', 'ep', 'tp')), parts along dimension 0, may hold values from -6 to 6
- norm_gain: float32 [4096], replicated, may hold values from 0.1 to 1.9
- route_ids: int32 [1536, 2], P(('grp', 'ep')), parts along dimension 0, may hold values from 0 to 3, all different within a row; in each aligned block of 48 rows (0 to 47, 48 to 95, ...) at most 48 rows name the same one
- route_weights: float32 [1536, 2], P(('grp', 'ep')), parts along dimension 0, may hold values from 0.25 to 1.25
- gate_weight: bfloat16 [4, 4096, 1024], P('ep', None, 'tp'), may hold values from -0.09375 to 0.09375
- up_weight: bfloat16 [4, 4096, 1024], P('ep', None, 'tp'), may hold values from -0.09375 to 0.09375
- down_weight: bfloat16 [4, 1024, 4096], P('ep', None, 'tp'), may hold values from -0.1875 to 0.1875
- shared_gate: bfloat16 [4096, 512], P(None, 'tp'), may hold values from -0.09375 to 0.09375
- shared_up: bfloat16 [4096, 512], P(None, 'tp'), may hold values from -0.09375 to 0.09375
- shared_down: bfloat16 [512, 4096], P(None, 'tp'), may hold values from -0.25 to 0.25
Outputs:
- mixer_output: bfloat16 [1536, 4096], P(('grp', 'ep'), 'tp'), parts along dimension 0
- expert_output: bfloat16 [1536, 4096], P(('grp', 'ep'), 'tp'), parts along dimension 0
There are 2 independent parts, one for each index of `grp`. A program takes and returns all parts, laid end to end along the dimension named above; an argument that names none is the same for every part. Nothing has to cross between parts.
Inputs may be any that keep to these rules, and one draw needn't show every extreme that they name: `route_ids`: the 2 entries of a row differ. In each aligned block of 48 rows (the routed tokens of one device) no expert is named by more than 48 rows, and in some block an expert is named by exactly 48 rows.
All inputs are finite; a program needn't handle non-finite values.
Results may differ from a plain program's by a relative error of at most 0.0067.
Values may be sent and summed in bfloat16 or wider, within the bound.
A program may use at most 64 MiB of HBM per device.

v0:
```python
import jax
import jax.numpy as jnp
from jax import lax
from jax.sharding import PartitionSpec as P

norm_floor = 0.5


def shifted(value, axis, steps):
    count = lax.axis_size(axis)
    leading, last = (max(0, -steps), min(count, count - steps))
    return lax.ppermute(value, axis, [(source, source + steps) for source in range(leading, last)])


def layer_norm(tokens, norm_gain):
    widened = tokens.astype(jnp.float32)
    centred = widened - jnp.mean(widened, axis=-1, keepdims=True)
    spread = jnp.mean(centred * centred, axis=-1, keepdims=True)
    return (centred * lax.rsqrt(spread + norm_floor) * norm_gain).astype(jnp.bfloat16)


def expert_hidden(inputs, gate_part, up_part):
    gate_value = jnp.dot(inputs, gate_part, preferred_element_type=jnp.float32)
    up_value = jnp.dot(inputs, up_part, preferred_element_type=jnp.float32)
    return (jax.nn.silu(gate_value) * up_value).astype(jnp.bfloat16)


def slot_ranks(route_ids, experts, lanes):
    tok_count, top_count = route_ids.shape
    grouped = route_ids.reshape(lanes, tok_count // lanes * top_count)
    onehot = (grouped[:, :, None] == jnp.arange(experts, dtype=jnp.int32)[None, None, :]).astype(
        jnp.int32
    )
    before = jnp.cumsum(onehot, axis=1) - onehot
    return jnp.sum(before * onehot, axis=2).reshape(tok_count, top_count)


def local(
    out_gate,
    in_gate,
    values,
    conv_taps,
    mixer_weight,
    expert_input,
    norm_gain,
    route_ids,
    route_weights,
    gate_weight,
    up_weight,
    down_weight,
    shared_gate,
    shared_up,
    shared_down,
):
    experts = lax.axis_size("ep")
    lanes = lax.axis_size("tp")
    lane_rows = expert_input.shape[0]
    width = expert_input.shape[1]
    tok_count, top_count = route_ids.shape
    capacity = (2 * lane_rows * top_count + experts - 1) // experts
    gated_values = (in_gate.astype(jnp.float32) * values.astype(jnp.float32)).astype(jnp.bfloat16)
    previous = shifted(gated_values[-2:], "ep", 1)
    extended = jnp.concatenate([previous, gated_values], axis=0).astype(jnp.float32)
    conv_state = (
        conv_taps[0] * extended[:-2] + conv_taps[1] * extended[1:-1] + conv_taps[2] * extended[2:]
    )
    mixed_rows = (out_gate.astype(jnp.float32) * conv_state).astype(jnp.bfloat16)
    normed_own = layer_norm(expert_input, norm_gain)
    mixed_whole, normed_rows = (
        lax.all_gather(mixed_rows, "tp", axis=1, tiled=True),
        lax.all_gather(normed_own, "tp", axis=0, tiled=True),
    )
    mixer_output = jnp.dot(mixed_whole, mixer_weight, preferred_element_type=jnp.float32).astype(
        jnp.bfloat16
    )
    shared_part = expert_hidden(normed_rows, shared_gate, shared_up)
    slot_index = slot_ranks(route_ids, experts, lanes)
    lane_of_row = (jnp.arange(tok_count, dtype=jnp.int32) // lane_rows)[:, None]
    positions = (route_ids * lanes + lane_of_row) * capacity + slot_index
    lane_index = lax.axis_index("tp")
    lane_ids = lax.dynamic_slice_in_dim(route_ids, lane_index * lane_rows, lane_rows, 0)
    lane_slots = lax.dynamic_slice_in_dim(slot_index, lane_index * lane_rows, lane_rows, 0)
    lane_places = lane_ids * capacity + lane_slots
    local_rows = jnp.broadcast_to(jnp.arange(lane_rows, dtype=jnp.int32)[:, None], lane_ids.shape)
    owners = jnp.full((experts * capacity,), lane_rows, jnp.int32)
    owners = owners.at[lane_places.reshape(-1)].set(local_rows.reshape(-1))
    outgoing = jnp.take(normed_own, owners, axis=0, mode="fill", fill_value=0)
    arrived = lax.all_to_all(
        outgoing.reshape(experts, capacity, width), "ep", split_axis=0, concat_axis=0, tiled=True
    )
    segment = lax.all_gather(arrived[None], "tp", axis=0, tiled=True)
    hidden_rows = expert_hidden(segment.reshape(-1, width), gate_weight[0], up_weight[0])
    spread_hidden = hidden_rows.reshape(segment.shape[:-1] + (hidden_rows.shape[-1],))
    routed_hidden = jnp.swapaxes(spread_hidden, 0, 1).reshape(-1, spread_hidden.shape[-1])
    routed_whole, shared_whole = (
        lax.all_gather(routed_hidden, "tp", axis=1, tiled=True),
        lax.all_gather(shared_part, "tp", axis=1, tiled=True),
    )
    routed_result = jnp.dot(
        routed_whole, down_weight[0], preferred_element_type=jnp.float32
    ).astype(jnp.bfloat16)
    out_cols = routed_result.shape[-1]
    returned = lax.all_to_all(
        routed_result.reshape(experts, lanes * capacity, out_cols),
        "ep",
        split_axis=0,
        concat_axis=0,
        tiled=True,
    )
    shared_result = jnp.dot(shared_whole, shared_down, preferred_element_type=jnp.float32)
    picked = jnp.take(
        returned.reshape(experts * lanes * capacity, out_cols), positions.reshape(-1), axis=0
    )
    picked = picked.astype(jnp.float32).reshape(tok_count, top_count, out_cols)
    expert_output = (shared_result + jnp.sum(route_weights[:, :, None] * picked, axis=1)).astype(
        jnp.bfloat16
    )
    return (mixer_output, expert_output)


def solution(mesh):
    placed = (
        P(("grp", "ep"), "tp"),
        P(("grp", "ep"), "tp"),
        P(("grp", "ep"), "tp"),
        P(None, "tp"),
        P(None, "tp"),
        P(("grp", "ep", "tp"), None),
        P(),
        P(("grp", "ep"), None),
        P(("grp", "ep"), None),
        P("ep", None, "tp"),
        P("ep", None, "tp"),
        P("ep", None, "tp"),
        P(None, "tp"),
        P(None, "tp"),
        P(None, "tp"),
    )
    return jax.shard_map(
        local,
        mesh=mesh,
        in_specs=placed,
        out_specs=(P(("grp", "ep"), "tp"), P(("grp", "ep"), "tp")),
        check_vma=False,
    )
```

profile of v0, /device:TPU:0, one launch (start us, length us, event | category | flops | bytes accessed | tf_op | source)
XLA Modules:
  0.0 200.9 jit_solution(447766201770005655)
XLA Ops:
  7.2 0.0 all-gather.12.cloned.1.call-start
  7.3 0.9 copy.37
  8.2 0.1 eq.15
  8.3 0.1 fusion.26
  8.5 0.2 reduce_window_sum.11
  8.7 0.2 select_reduce_fusion
  8.9 0.1 reshape.139
  9.1 0.1 reshape.140
  9.2 0.1 reshape.168
  9.3 0.9 scatter_custom_fusion
  10.2 1.2 convert_reduce_fusion
  11.4 0.3 fusion.19
  11.7 0.1 broadcast_in_dim.43
  11.8 0.2 fusion.21
  12.0 2.7 %gather_fusion = bf16[192,4096]{1,0:T(8,128)(2,1)} fusion(bf16[48,4096]{1,0:T(8,128)(2,1)S(1)} %fusion.21, s32[1024]{0:T(1024)S(1)} %pad_clamp_fusion.1), kind=kCustom, calls=%fused_computation | custom fusion | bytes 3146496 | tf_op jit(solution)/shard_map/jit(_take)/gather | solution.py:87
  14.7 1.6 broadcast_select_fusion
  16.3 43.2 %all_to_all.10 = bf16[4,48,4096]{2,1,0:T(8,128)(2,1)} all-to-all(bf16[4,48,4096]{2,1,0:T(8,128)(2,1)S(1)} %broadcast_select_fusion), channel_id=1, replica_groups=mesh['grp'=2,'ep'=4,'tp'=4] {'ep'}, dimensions={0} | all-to-all | bytes 3145728 | tf_op jit(solution)/shard_map/all_to_all | solution.py:88
  59.5 0.0 all-gather.10.cloned.1.call-start
  59.6 45.6 %all-gather.12.cloned.1.call-done = bf16[16,48,4096]{2,1,0:T(8,128)(2,1)} async-done(((bf16[4,48,4096]{2,1,0:T(8,128)(2,1)}), bf16[16,48,4096]{2,1,0:T(8,128)(2,1)}) %all-gather.12.cloned.1.call-update) | async-done | bytes 6291472 | tf_op jit(solution)/shard_map/all_gather | solution.py:91
  105.2 5.4 %fusion.4 = f32[768,256]{1,0:T(8,128)S(1)} fusion(bf16[768,4096]{1,0:T(8,128)(2,1)} %bitcast.46, bf16[1,4096,256]{2,1,0:T(8,128)(2,1)} %param.24), kind=kOutput, calls=%fused_computation.7 | convolution fusion | flops 1610612736 | bytes 9175040 | tf_op jit(solution)/shard_map/dot_general | solution.py:23
  110.6 0.4 copy-done.13
  111.0 1.8 fusion.12
  112.8 0.8 copy.41
  113.6 0.0 all-gather.8.cloned.1.call-start
  113.7 0.7 all-gather.8.cloned.1.call-update
  114.4 1.1 multiply_convert_fusion
  115.6 3.4 %collective-permute-start = (bf16[2,1024]{1,0:T(2,128)(2,1)S(1)}, bf16[2,1024]{1,0:T(2,128)(2,1)S(1)}, u32[]{:S(2)}, u32[]{:S(2)}) collective-permute-start(bf16[2,1024]{1,0:T(2,128)(2,1)S(1)} %slice.32), channel_id=1, source_target_pairs={{0,4},{4,8},{8,12},{1,5},{5,9},{9,13},{2,6},{6,10},{10,14},{3,7},{... | collective-permute-start | bytes 12296 | tf_op jit(solution)/shard_map/ppermute | solution.py:12
  119.0 1.3 collective-permute-done
  120.3 0.1 maximum_convert_fusion
  120.4 1.0 fusion.24
  121.5 12.1 %all-gather.10.cloned.1.call-done = bf16[768,1024]{1,0:T(8,128)(2,1)} async-done(((bf16[768,256]{1,0:T(8,128)(2,1)}), bf16[768,1024]{1,0:T(8,128)(2,1)}) %all-gather.10.cloned.1.call-update) | async-done | bytes 1572880 | tf_op jit(solution)/shard_map/all_gather | solution.py:96
  133.6 4.4 %fusion.6 = bf16[768,1024]{1,0:T(8,128)(2,1)} fusion(bf16[768,1024]{1,0:T(8,128)(2,1)} %all-gather.10.cloned.1.call-done, bf16[1,1024,1024]{2,1,0:T(8,128)(2,1)S(1)} %copy-done), kind=kOutput, calls=%fused_computation.9 | convolution fusion | flops 1611399168 | bytes 5242880 | tf_op jit(solution)/shard_map/dot_general | solution.py:99
  138.0 4.7 %all-to-all-start.1 = ((bf16[4,192,1024]{2,1,0:T(8,128)(2,1)}), bf16[4,192,1024]{2,1,0:T(8,128)(2,1)}, u32[]{:S(2)}, u32[]{:S(2)}) async-start(bf16[4,192,1024]{2,1,0:T(8,128)(2,1)} %bitcast.40), calls=%async_computation.1 | async-start | bytes 3145728 | tf_op jit(solution)/shard_map/all_to_all | solution.py:103
  142.7 0.1 copy.38
  142.8 0.1 copy.42
  143.0 0.1 reshape.147
  143.1 0.2 copy.39
  143.3 0.1 copy.36
  143.4 11.4 %all-gather.8.cloned.1.call-done = bf16[192,4096]{1,0:T(8,128)(2,1)} async-done(((bf16[48,4096]{1,0:T(8,128)(2,1)}), bf16[192,4096]{1,0:T(8,128)(2,1)}) %all-gather.8.cloned.1.call-update) | async-done | bytes 1572880 | tf_op jit(solution)/shard_map/all_gather | solution.py:71
  154.8 2.1 %fusion.32 = f32[192,128]{1,0:T(8,128)S(1)} fusion(bf16[192,4096]{1,0:T(8,128)(2,1)} %all-gather.8.cloned.1.call-done, bf16[4096,128]{1,0:T(8,128)(2,1)S(1)} %copy-done.5), kind=kOutput, calls=%fused_computation.60 | convolution fusion | flops 201326592 | bytes 2719744 | tf_op jit(solution)/shard_map/dot_general | solution.py:23
  157.0 0.6 fusion.16
  157.6 5.8 %all_gather.17 = bf16[192,512]{1,0:T(8,128)(2,1)S(1)} all-gather(bf16[192,128]{1,0:T(8,128)(2,1)S(1)} %fusion.16), channel_id=1, replica_groups=mesh['grp'=2,'ep'=4,'tp'=4] {'tp'}, dimensions={1}, use_global_device_ids=true | all-gather | bytes 245760 | tf_op jit(solution)/shard_map/all_gather | solution.py:97
  163.4 13.1 %all-gather.6.cloned.1.call-done = bf16[192,4096]{1,0:T(8,128)(2,1)} async-done(((bf16[192,1024]{1,0:T(8,128)(2,1)}), bf16[192,4096]{1,0:T(8,128)(2,1)}) %all-gather.6.cloned.1.call-update) | async-done | bytes 1572880 | tf_op jit(solution)/shard_map/all_gather | solution.py:70
  176.5 6.4 %convolution_convert_fusion = bf16[192,1024]{1,0:T(8,128)(2,1)} fusion(bf16[192,4096]{1,0:T(8,128)(2,1)} %all-gather.6.cloned.1.call-done, bf16[4096,1024]{1,0:T(8,128)(2,1)} %param.19), kind=kOutput, calls=%fused_computation.16 | convolution fusion | flops 1610809344 | bytes 10354688 | tf_op jit(solution)/shard_map/dot_general | solution.py:73
  182.9 5.0 %gather_fusion.1 = bf16[384,1024]{1,0:T(8,128)(2,1)} fusion(bf16[768,1024]{1,0:T(8,128)(2,1)} %bitcast.13, s32[1024]{0:T(1024)S(1)} %pad_clamp_fusion), kind=kCustom, calls=%fused_computation.1 | custom fusion | bytes 1574400 | tf_op jit(solution)/shard_map/jit(_take)/gather | solution.py:111
  187.9 2.1 %gather.15 = bf16[192,2,1024]{2,1,0:T(2,128)(2,1)S(1)} reshape(bf16[384,1024]{1,0:T(8,128)(2,1)} %gather_fusion.1) | data formatting | bytes 1572864 | tf_op jit(solution)/shard_map/jit(_take)/gather | solution.py:111
  190.1 3.1 %multiply_reduce_fusion = f32[192,1024]{1,0:T(8,128)S(1)} fusion(bf16[192,2,1024]{2,1,0:T(2,128)(2,1)S(1)} %gather.15, pred[192,2]{1,0:T(8,128)(4,1)S(1)} %copy.39, f32[192,2]{1,0:T(8,128)S(1)} %copy.36), kind=kLoop, calls=%fused_computation.10 | loop fusion | flops 1376256 | bytes 1574784 | tf_op jit(solution)/shard_map/reduce_sum | solution.py:115
  193.2 1.1 fusion.15
  (48 shorter events, 0.3 us)
Async XLA Ops:
  7.2 126.4 %copy-start = (bf16[1,1024,1024]{2,1,0:T(8,128)(2,1)S(1)}, bf16[1,1024,1024]{2,1,0:T(8,128)(2,1)}, u32[]{:S(2)}) copy-start(bf16[1,1024,1024]{2,1,0:T(8,128)(2,1)} %param.26) | copy-start | bytes 6291460
  7.2 4.2 %copy-start.2 = (bf16[48,4096]{1,0:T(8,128)(2,1)S(1)}, bf16[48,4096]{1,0:T(8,128)(2,1)}, u32[]{:S(2)}) copy-start(bf16[48,4096]{1,0:T(8,128)(2,1)} %param.20) | copy-start | bytes 1179652
  7.2 4.6 %copy-start.8 = (f32[4096]{0:T(1024)S(1)}, f32[4096]{0:T(1024)}, u32[]{:S(2)}) copy-start(f32[4096]{0:T(1024)} %param.21) | copy-start | bytes 49156
  7.2 98.0 %all-gather.12.cloned.1.call-start = ((), (), s32[]{:S(2)}) async-start(), calls=%async_computation.5 | async-start | bytes 7864320 | tf_op jit(solution)/shard_map/all_gather | solution.py:91
  12.0 2.7 %copy-start.1 = (bf16[48,4096]{1,0:T(8,128)(2,1)}, bf16[48,4096]{1,0:T(8,128)(2,1)S(1)}, u32[]{:S(2)}) copy-start(bf16[48,4096]{1,0:T(8,128)(2,1)S(1)} %fusion.21) | copy-start | bytes 1179652
  59.5 74.1 %all-gather.10.cloned.1.call-start = ((), (), s32[]{:S(2)}) async-start(), calls=%async_computation.4 | async-start | bytes 1966080 | tf_op jit(solution)/shard_map/all_gather | solution.py:96
  105.2 5.4 %copy-start.12 = (bf16[16,48,4096]{2,1,0:T(8,128)(2,1)S(1)}, bf16[16,48,4096]{2,1,0:T(8,128)(2,1)}, u32[]{:S(2)}) copy-start(bf16[16,48,4096]{2,1,0:T(8,128)(2,1)} %all-gather.12.cloned.1.call-done) | copy-start | bytes 18874372
  105.2 5.8 %copy-start.13 = (bf16[1,4096,256]{2,1,0:T(8,128)(2,1)S(1)}, bf16[1,4096,256]{2,1,0:T(8,128)(2,1)}, u32[]{:S(2)}) copy-start(bf16[1,4096,256]{2,1,0:T(8,128)(2,1)} %param.25) | copy-start | bytes 6291460
  112.8 1.6 copy-start.7
  112.8 6.2 %copy-start.9 = (f32[3,1024]{1,0:T(4,128)S(1)}, f32[3,1024]{1,0:T(4,128)}, u32[]{:S(2)}) copy-start(f32[3,1024]{1,0:T(4,128)} %param.18) | copy-start | bytes 36868
  113.6 6.8 %copy-start.6 = (bf16[192,1024]{1,0:T(8,128)(2,1)S(1)}, bf16[192,1024]{1,0:T(8,128)(2,1)}, u32[]{:S(2)}) copy-start(bf16[192,1024]{1,0:T(8,128)(2,1)} %param.15) | copy-start | bytes 1179652
  113.6 41.2 %all-gather.8.cloned.1.call-start = ((), (), s32[]{:S(2)}) async-start(), calls=%async_computation.3 | async-start | bytes 1966080 | tf_op jit(solution)/shard_map/all_gather | solution.py:71
  114.4 62.1 %all-gather.6.cloned.1.call-start = ((), (), s32[]{:S(2)}) async-start(), calls=%async_computation.2 | async-start | bytes 1966080 | tf_op jit(solution)/shard_map/all_gather | solution.py:70
  115.6 4.7 %collective-permute-start = (bf16[2,1024]{1,0:T(2,128)(2,1)S(1)}, bf16[2,1024]{1,0:T(2,128)(2,1)S(1)}, u32[]{:S(2)}, u32[]{:S(2)}) collective-permute-start(bf16[2,1024]{1,0:T(2,128)(2,1)S(1)} %slice.32), channel_id=1, source_target_pairs={{0,4},{4,8},{8,12},{1,5},{5,9},{9,13},{2,6},{6,10},{10,14},{3,7},{... | collective-permute-start | bytes 12296 | tf_op jit(solution)/shard_map/ppermute | solution.py:12
  138.0 4.8 %copy-start.10 = (s32[192,2]{0,1:T(2,128)S(1)}, s32[192,2]{0,1:T(2,128)}, u32[]{:S(2)}) copy-start(s32[192,2]{0,1:T(2,128)} %param.22) | copy-start | bytes 4612
  138.0 5.3 %copy-start.11 = (f32[192,2]{0,1:T(2,128)S(1)}, f32[192,2]{0,1:T(2,128)}, u32[]{:S(2)}) copy-start(f32[192,2]{0,1:T(2,128)} %param.23) | copy-start | bytes 4612
  138.0 16.9 %copy-start.5 = (bf16[4096,128]{1,0:T(8,128)(2,1)S(1)}, bf16[4096,128]{1,0:T(8,128)(2,1)}, u32[]{:S(2)}) copy-start(bf16[4096,128]{1,0:T(8,128)(2,1)} %param.27) | copy-start | bytes 3145732
  138.0 44.9 %all-to-all-start.1 = ((bf16[4,192,1024]{2,1,0:T(8,128)(2,1)}), bf16[4,192,1024]{2,1,0:T(8,128)(2,1)}, u32[]{:S(2)}, u32[]{:S(2)}) async-start(bf16[4,192,1024]{2,1,0:T(8,128)(2,1)} %bitcast.40), calls=%async_computation.1 | async-start | bytes 3145728 | tf_op jit(solution)/shard_map/all_to_all | solution.py:103
  154.8 2.1 %copy-start.3 = (bf16[192,4096]{1,0:T(8,128)(2,1)S(1)}, bf16[192,4096]{1,0:T(8,128)(2,1)}, u32[]{:S(2)}) copy-start(bf16[192,4096]{1,0:T(8,128)(2,1)} %all-gather.8.cloned.1.call-done) | copy-start | bytes 4718596
  154.8 2.2 %copy-start.14 = (bf16[4096,128]{1,0:T(8,128)(2,1)S(1)}, bf16[4096,128]{1,0:T(8,128)(2,1)}, u32[]{:S(2)}) copy-start(bf16[4096,128]{1,0:T(8,128)(2,1)} %param.28) | copy-start | bytes 3145732
  190.0 3.1 %copy-start.4 = (bf16[512,1024]{1,0:T(8,128)(2,1)S(1)}, bf16[512,1024]{1,0:T(8,128)(2,1)}, u32[]{:S(2)}) copy-start(bf16[512,1024]{1,0:T(8,128)(2,1)} %param.29) | copy-start | bytes 3145732
Sparse Core Ops, SparseCore 0:
  59.6 45.4 all-gather.11
  113.8 19.8 all-gather.9
  135.2 19.6 all-gather.7
  156.8 19.6 all-gather.5
where the time goes:
time: 201 us
  waiting for transfers between devices  84.3 us (42%)
  blocking collectives  49 us (24%)
  matrix products  21.7 us (11%)
  local copies, waits for them, and re-layouts  14.2 us (7%)
  between operations  14.1 us (7%)
  other arithmetic  9.27 us (5%)
  starting transfers between devices  8.28 us (4%)
    all_gather x1, waiting for transfers between devices, local(): segment = lax.all_gather(arrived[None], 'tp', axis=0, tiled=True)  45.6 us
    all_to_all x1, blocking collectives, local(): lax.all_to_all(outgoing.reshape(experts, capacity, width), 'ep', split_ax...  43.2 us
    all_gather x1, waiting for transfers between devices, local(): lax.all_gather(mixed_rows, 'tp', axis=1, tiled=True)  13.1 us
    all_gather x1, waiting for transfers between devices, local(): lax.all_gather(routed_hidden, 'tp', axis=1, tiled=True)  12.1 us
    all_gather x1, waiting for transfers between devices, local(): lax.all_gather(normed_own, 'tp', axis=0, tiled=True)  11.4 us
    dot_general x2, matrix products, expert_hidden(): gate_value = jnp.dot(inputs, gate_part, preferred_element_type=jnp.float32)  7.47 us
    gather x2, local copies, waits for them, and re-layouts, local(): jnp.take(returned.reshape(experts * lanes * capacity, out_cols), position...  7.12 us
    dot_general x1, matrix products, local(): jnp.dot(mixed_whole, mixer_weight, preferred_element_type=jnp.float32)  6.41 us
  transfers between devices with their start and end apart: 6, of which 5 were waited for; matrix products, arithmetic and copies ran while one was open for 8% of the time, Pallas kernels for 0%

commit v1 on v0

--- a/solution.py
+++ b/solution.py
@@ -1,7 +1,15 @@
+import functools
+
 import jax
 import jax.numpy as jnp
 from jax import lax
+from jax.experimental import pallas as pl
+from jax.experimental.pallas import tpu as pltpu
 from jax.sharding import PartitionSpec as P
+
+MESH = pl.DeviceIdType.MESH
+CORES = 2
+TILE = 256
 
 norm_floor = 0.5
 
@@ -35,7 +43,7 @@
     return jnp.sum(before * onehot, axis=2).reshape(tok_count, top_count)
 
 
-def local(
+def plain(
     out_gate,
     in_gate,
     values,
@@ -118,6 +126,434 @@
     return (mixer_output, expert_output)
 
 
+def silu_product(gate_value, up_value):
+    return (gate_value * (1.0 / (1.0 + jnp.exp(-gate_value))) * up_value).astype(jnp.bfloat16)
+
+
+def dot32(left, right):
+    return jnp.dot(left, right, preferred_element_type=jnp.float32)
+
+
+def kernel(
+    n_ep,
+    n_tp,
+    ids,
+    rw,
+    og_h,
+    ig_h,
+    va_h,
+    taps_h,
+    mw_h,
+    ei_h,
+    ng_h,
+    gw_h,
+    uw_h,
+    dw_h,
+    sg_h,
+    su_h,
+    sd_h,
+    mix_out,
+    exp_out,
+    og,
+    ig,
+    va,
+    taps,
+    mw,
+    ei,
+    ng,
+    gw,
+    uw,
+    dw,
+    sg,
+    su,
+    sd,
+    tok,
+    hid,
+    shd,
+    mixed,
+    gated,
+    halo,
+    res,
+    ret,
+    ld,
+    z_send,
+    z_recv,
+    x_send,
+    x_recv,
+    p_send,
+    p_recv,
+    r_send,
+    r_recv,
+    h_sem,
+):
+    e = lax.axis_index("ep")
+    t = lax.axis_index("tp")
+    n_x = n_tp // CORES
+    partner = t + 1 - 2 * (t % CORES)
+    lane_rows, width = ei.shape
+    rows, chans = og.shape
+
+    loads = {}
+    for number, (name, src, dst) in enumerate(
+        (
+            ("ei", ei_h, ei),
+            ("ng", ng_h, ng),
+            ("ig", ig_h, ig),
+            ("va", va_h, va),
+            ("og", og_h, og),
+            ("taps", taps_h, taps),
+            ("gw", gw_h, gw),
+            ("uw", uw_h, uw),
+            ("sg", sg_h, sg),
+            ("su", su_h, su),
+            ("dw", dw_h, dw),
+            ("sd", sd_h, sd),
+            ("mw", mw_h, mw),
+        )
+    ):
+        loads[name] = pltpu.make_async_copy(src, dst, ld.at[number])
+        loads[name].start()
+
+    barrier = pltpu.get_barrier_semaphore()
+    greeted = [{"ep": (e + d) % n_ep, "tp": t} for d in range(1, n_ep)]
+    greeted += [{"ep": e, "tp": (t + CORES * d) % n_tp} for d in range(1, n_x)]
+    greeted += [{"ep": e, "tp": partner}]
+    for peer in greeted:
+        pl.semaphore_signal(barrier, inc=1, device_id=peer, device_id_type=MESH)
+
+    def remote(src, dst, send, recv, ep, tp):
+        return pltpu.make_async_remote_copy(
+            src_ref=src,
+            dst_ref=dst,
+            send_sem=send,
+            recv_sem=recv,
+            device_id={"ep": ep, "tp": tp},
+            device_id_type=MESH,
+        )
+
+    def cross(slot, g, d, lane):
+        return remote(
+            slot(lane), slot(lane), x_send.at[g, d - 1], x_recv.at[g, d - 1],
+            e, (t + CORES * d) % n_tp,
+        )
+
+    def across(slot, g, d, lane):
+        return remote(slot(lane), slot(lane), p_send.at[g, d], p_recv.at[g, d], e, partner)
+
+    def from_x(d):
+        return (t + n_tp - CORES * d) % n_tp
+
+    def from_partner(d):
+        return (partner + n_tp - CORES * d) % n_tp
+
+    def gather_start(slot, g):
+        for d in range(1, n_x):
+            cross(slot, g, d, t).start()
+        across(slot, g, 0, t).start()
+
+    def gather_forward(slot, g):
+        for d in range(1, n_x):
+            cross(slot, g, d, from_x(d)).wait_recv()
+            across(slot, g, d, from_x(d)).start()
+
+    def gather_finish(slot, g):
+        for d in range(n_x):
+            across(slot, g, d, from_partner(d)).wait_recv()
+
+    def gather_drain(slot, g):
+        for d in range(1, n_x):
+            cross(slot, g, d, t).wait_send()
+            across(slot, g, d, from_x(d)).wait_send()
+        across(slot, g, 0, t).wait_send()
+
+    shared_g, mixed_g = 2 * n_ep, 2 * n_ep + 1
+
+    def tok_slot(j):
+        return lambda lane: tok.at[j, lane]
+
+    def hid_slot(j):
+        return lambda lane: hid.at[j, lane]
+
+    def shd_slot(lane):
+        return shd.at[lane]
+
+    def mixed_slot(lane):
+        return mixed.at[lane]
+
+    nearest = jnp.minimum(e, n_ep - 1 - e)
+    left_short = e <= n_ep - 1 - e
+
+    def block_at(k):
+        near = jnp.where(k % 2 == 1, e - (k + 1) // 2, e + k // 2)
+        far = jnp.where(left_short, k, n_ep - 1 - k)
+        return jnp.where(k <= 2 * nearest, near, far)
+
+    def z_right(j):
+        return remote(tok.at[j, t], tok.at[j, t], z_send.at[0, j], z_recv.at[j],
+                      jnp.minimum(e + 1, n_ep - 1), t)
+
+    def z_left(j):
+        return remote(tok.at[j, t], tok.at[j, t], z_send.at[1, j], z_recv.at[j],
+                      jnp.maximum(e - 1, 0), t)
+
+    def goes_right(j):
+        return (j <= e) & (e < n_ep - 1)
+
+    def goes_left(j):
+        return (j >= e) & (e > 0)
+
+    def spread(k):
+        j = block_at(k)
+
+        @pl.when(k > 0)
+        def _():
+            z_right(j).wait_recv()
+
+        @pl.when(goes_right(j))
+        def _():
+            z_right(j).start()
+
+        @pl.when(goes_left(j))
+        def _():
+            z_left(j).start()
+
+        gather_start(tok_slot(j), j)
+
+    def back(j):
+        return remote(res.at[j], ret.at[e], r_send.at[j], r_recv.at[e], j, t)
+
+    loads["ei"].wait()
+    loads["ng"].wait()
+
+    def norm_rows(r, _):
+        at = pl.ds(pl.multiple_of(r * 16, 16), 16)
+        widened = ei[at, :].astype(jnp.float32)
+        centred = widened - jnp.mean(widened, axis=-1, keepdims=True)
+        spread_of = jnp.mean(centred * centred, axis=-1, keepdims=True)
+        normed = centred * lax.rsqrt(spread_of + norm_floor) * ng[...]
+        tok[e, t, at, :] = normed.astype(jnp.bfloat16)
+        return 0
+
+    lax.fori_loop(0, lane_rows // 16, norm_rows, 0)
+    pl.semaphore_wait(barrier, len(greeted))
+    spread(0)
+
+    loads["ig"].wait()
+    loads["va"].wait()
+
+    def gate_cols(c, _):
+        at = pl.ds(pl.multiple_of(c * 128, 128), 128)
+        gated[:, at] = (ig[:, at].astype(jnp.float32) * va[:, at].astype(jnp.float32)).astype(
+            jnp.bfloat16
+        )
+        return 0
+
+    lax.fori_loop(0, chans // 128, gate_cols, 0)
+
+    def halo_copy():
+        return remote(gated.at[pl.ds(rows - 16, 16)], halo, h_sem.at[0], h_sem.at[1],
+                      jnp.minimum(e + 1, n_ep - 1), t)
+
+    @pl.when(e < n_ep - 1)
+    def _():
+        halo_copy().start()
+
+    loads["og"].wait()
+    loads["taps"].wait()
+
+    @pl.when(e == 0)
+    def _():
+        halo[...] = jnp.zeros_like(halo)
+
+    @pl.when(e > 0)
+    def _():
+        halo_copy().wait_recv()
+
+    def mix_cols(c, _):
+        at = pl.ds(pl.multiple_of(c * 128, 128), 128)
+        now = gated[:, at].astype(jnp.float32)
+        before = halo[:, at].astype(jnp.float32)
+        place = lax.broadcasted_iota(jnp.int32, now.shape, 0)
+        one = jnp.where(place == 0, before[15:16], pltpu.roll(now, 1, 0))
+        two = jnp.where(
+            place == 0, before[14:15], jnp.where(place == 1, before[15:16], pltpu.roll(now, 2, 0))
+        )
+        state = taps[0:1, at] * two + taps[1:2, at] * one + taps[2:3, at] * now
+        mixed[t, :, at] = (og[:, at].astype(jnp.float32) * state).astype(jnp.bfloat16)
+        return 0
+
+    lax.fori_loop(0, chans // 128, mix_cols, 0)
+    for name in ("gw", "uw", "sg", "su"):
+        loads[name].wait()
+
+    def step(s, _):
+        @pl.when(s + 1 < n_ep)
+        def _():
+            spread(s + 1)
+
+        @pl.when(s < n_ep)
+        def _():
+            j = block_at(s)
+            gather_forward(tok_slot(j), j)
+            gather_finish(tok_slot(j), j)
+            block = tok[j].reshape(rows, width)
+            hid[j, t] = silu_product(dot32(block, gw[...]), dot32(block, uw[...]))
+            gather_start(hid_slot(j), n_ep + j)
+
+        @pl.when(s == 0)
+        def _():
+            block = tok[e].reshape(rows, width)
+            shd[t] = silu_product(dot32(block, sg[...]), dot32(block, su[...]))
+            gather_start(shd_slot, shared_g)
+            loads["dw"].wait()
+
+        @pl.when(s == n_ep - 1)
+        def _():
+            gather_start(mixed_slot, mixed_g)
+
+        @pl.when(s >= 1)
+        def _():
+            j = block_at(s - 1)
+            gather_forward(hid_slot(j), n_ep + j)
+            gather_finish(hid_slot(j), n_ep + j)
+            part = hid.shape[-1]
+            for c in range(chans // TILE):
+                at = slice(c * TILE, (c + 1) * TILE)
+                total = dot32(hid[j, 0], dw[0:part, at])
+                for lane in range(1, n_tp):
+                    total += dot32(hid[j, lane], dw[lane * part : (lane + 1) * part, at])
+                res[j, :, at] = total.astype(jnp.bfloat16)
+
+            @pl.when(j != e)
+            def _():
+                back(j).start()
+
+        return 0
+
+    lax.fori_loop(0, n_ep + 1, step, 0)
+
+    gather_forward(shd_slot, shared_g)
+    gather_forward(mixed_slot, mixed_g)
+    gather_finish(shd_slot, shared_g)
+    loads["sd"].wait()
+    loads["mw"].wait()
+    gather_finish(mixed_slot, mixed_g)
+
+    def mixer_cols(c, _):
+        at = pl.ds(pl.multiple_of(c * TILE, TILE), TILE)
+        total = dot32(mixed[0], mw[0:chans, at])
+        for lane in range(1, n_tp):
+            total += dot32(mixed[lane], mw[lane * chans : (lane + 1) * chans, at])
+        mix_out[:, at] = total.astype(jnp.bfloat16)
+        return 0
+
+    lax.fori_loop(0, chans // TILE, mixer_cols, 0)
+
+    for d in range(1, n_ep):
+        i = (e + d) % n_ep
+        remote(res.at[i], ret.at[i], r_send.at[i], r_recv.at[i], i, t).wait_recv()
+
+    def combine_cols(c, _):
+        at = pl.ds(pl.multiple_of(c * TILE, TILE), TILE)
+        part = shd.shape[-1]
+        total = dot32(shd[0], sd[0:part, at])
+        for lane in range(1, n_tp):
+            total += dot32(shd[lane], sd[lane * part : (lane + 1) * part, at])
+        for d in range(n_ep):
+            i = (e + d) % n_ep
+            weight = jnp.sum(jnp.where(ids[...] == i, rw[...], 0.0), axis=1, keepdims=True)
+            found = res[e, :, at] if d == 0 else ret[i, :, at]
+            total += weight * found.astype(jnp.float32)
+        exp_out[:, at] = total.astype(jnp.bfloat16)
+        return 0
+
+    lax.fori_loop(0, chans // TILE, combine_cols, 0)
+
+    @pl.when(e < n_ep - 1)
+    def _():
+        halo_copy().wait_send()
+
+    def drain(j, _):
+        @pl.when(goes_right(j))
+        def _():
+            z_right(j).wait_send()
+
+        @pl.when(goes_left(j))
+        def _():
+            z_left(j).wait_send()
+
+        gather_drain(tok_slot(j), j)
+        gather_drain(hid_slot(j), n_ep + j)
+
+        @pl.when(j != e)
+        def _():
+            back(j).wait_send()
+
+        return 0
+
+    lax.fori_loop(0, n_ep, drain, 0)
+    gather_drain(shd_slot, shared_g)
+    gather_drain(mixed_slot, mixed_g)
+
+
+def joined(n_ep, n_tp, *args):
+    (og, ig, va, taps, mw, ei, ng, ids, rw, gw, uw, dw, sg, su, sd) = args
+    gw, uw, dw, ng = gw[0], uw[0], dw[0], ng[None]
+    bf, f32 = jnp.bfloat16, jnp.float32
+    rows, chans = og.shape
+    lane_rows, width = ei.shape
+    n_x = n_tp // CORES
+    sems = 2 * n_ep + 2
+    big = (og, ig, va, taps, mw, ei, ng, gw, uw, dw, sg, su, sd)
+    out = jax.ShapeDtypeStruct((rows, chans), bf)
+    vmem = pl.BlockSpec(memory_space=pltpu.VMEM)
+    dma = pltpu.SemaphoreType.DMA
+    return pl.pallas_call(
+        functools.partial(kernel, n_ep, n_tp),
+        out_shape=(out, out),
+        in_specs=[vmem, vmem] + [pl.BlockSpec(memory_space=pl.ANY)] * len(big),
+        out_specs=(vmem, vmem),
+        scratch_shapes=[pltpu.VMEM(a.shape, a.dtype) for a in big]
+        + [
+            pltpu.VMEM((n_ep, n_tp, lane_rows, width), bf),
+            pltpu.VMEM((n_ep, n_tp, rows, gw.shape[-1]), bf),
+            pltpu.VMEM((n_tp, rows, sg.shape[-1]), bf),
+            pltpu.VMEM((n_tp, rows, chans), bf),
+            pltpu.VMEM((rows, chans), bf),
+            pltpu.VMEM((16, chans), bf),
+            pltpu.VMEM((n_ep, rows, chans), bf),
+            pltpu.VMEM((n_ep, rows, chans), bf),
+            dma((len(big),)),
+            dma((2, n_ep)),
+            dma((n_ep,)),
+            dma((sems, max(1, n_x - 1))),
+            dma((sems, max(1, n_x - 1))),
+            dma((sems, n_x)),
+            dma((sems, n_x)),
+            dma((n_ep,)),
+            dma((n_ep,)),
+            dma((2,)),
+        ],
+        compiler_params=pltpu.CompilerParams(
+            collective_id=0, has_side_effects=True, vmem_limit_bytes=60 * 1024 * 1024
+        ),
+    )(ids, rw, *big)
+
+
+def local(*args):
+    n_ep, n_tp = lax.axis_size("ep"), lax.axis_size("tp")
+    chans, lane_rows = args[0].shape[1], args[5].shape[0]
+    aligned = (
+        n_tp % CORES == 0
+        and lane_rows % 16 == 0
+        and lane_rows * n_tp == args[0].shape[0]
+        and chans % TILE == 0
+        and args[9].shape[2] % 128 == 0
+        and args[12].shape[1] % 128 == 0
+    )
+    return joined(n_ep, n_tp, *args) if aligned else plain(*args)
+
+
 def solution(mesh):
     placed = (
         P(("grp", "ep"), "tp"),

time: 201 us -> 96.6 us (0.48)
  the two profiles are of different devices: /device:TPU:0 before, /device:TPU:24 now
where the time goes in v1:
time: 96.6 us; the launch traced here: 96.4 us
  Pallas kernels  89.3 us (92%)
  local copies, waits for them, and re-layouts  6.42 us (7%)
    pallas_call x1, Pallas kernels, joined(): pl.pallas_call(functools.partial(kernel, n_ep, n_tp), out_shape=(out, out...  89.3 us
    unnamed x4, local copies, waits for them, and re-layouts  6.42 us

profile of v1, /device:TPU:24, one launch (start us, length us, event | category | flops | bytes accessed | tf_op | source)
XLA Modules:
  0.0 96.4 jit_solution(10800764890199702125)
XLA Ops:
  0.6 1.4 %copy.17.ids = s32[192,2]{1,0:T(8,128)} copy(s32[192,2]{0,1:T(2,128)} %param.22) | data formatting | bytes 3072 | tf_op args[7]
  2.1 1.4 %copy.18.rw = f32[192,2]{1,0:T(8,128)} copy(f32[192,2]{0,1:T(2,128)} %param.23) | data formatting | bytes 3072 | tf_op args[8]
  3.5 89.3 %shard_map.158 = (bf16[192,1024]{1,0:T(8,128)(2,1)}, bf16[192,1024]{1,0:T(8,128)(2,1)}) custom-call(s32[192,2]{1,0:T(8,128)} %copy.17.ids, f32[192,2]{1,0:T(8,128)} %copy.18.rw, bf16[192,1024]{1,0:T(8,128)(2,1)} %og_h.1, bf16[192,1024]{1,0:T(8,128)(2,1)} %ig_h.1, bf16[192,1024]{1,0:T(8,128)(2,1)} %va_h.1, f32[3,1024]{1,0:T(4,128)} %taps_h.1, ...), custom_call_target="tpu_custom_call" | custom-call | tf_op jit(solution)/shard_map/pallas_call | solution.py:511
  92.8 1.8 %copy.21 = bf16[192,1024]{1,0:T(8,128)(2,1)} copy(bf16[192,1024]{1,0:T(8,128)(2,1)} %get-tuple-element.4) | data formatting | bytes 786432
  94.6 1.8 %copy.22 = bf16[192,1024]{1,0:T(8,128)(2,1)} copy(bf16[192,1024]{1,0:T(8,128)(2,1)} %get-tuple-element.5) | data formatting | bytes 786432

commit v2 on v1

--- a/solution.py
+++ b/solution.py
@@ -10,6 +10,7 @@
 MESH = pl.DeviceIdType.MESH
 CORES = 2
 TILE = 256
+CHUNKS = 4
 
 norm_floor = 0.5
 
@@ -174,7 +175,8 @@
     gated,
     halo,
     res,
-    ret,
+    pin,
+    wts,
     ld,
     z_send,
     z_recv,
@@ -184,6 +186,8 @@
     p_recv,
     r_send,
     r_recv,
+    w_send,
+    w_recv,
     h_sem,
 ):
     e = lax.axis_index("ep")
@@ -319,8 +323,31 @@
 
         gather_start(tok_slot(j), j)
 
-    def back(j):
-        return remote(res.at[j], ret.at[e], r_send.at[j], r_recv.at[e], j, t)
+    piece = rows // CHUNKS
+
+    def hop(j, c):
+        at = pl.ds(pl.multiple_of(c * piece, 16), piece)
+        after = jnp.clip(jnp.where(j > e, e + 1, e - 1), 0, n_ep - 1)
+        slot = jnp.where((j < e) & (after == j), n_ep, j)
+        return remote(res.at[j, at], pin.at[slot, at], r_send.at[j, c], r_recv.at[slot, c], after, t)
+
+    def hop_arrives(slot, c):
+        at = pl.ds(pl.multiple_of(c * piece, 16), piece)
+        remote(res.at[0, at], pin.at[slot, at], r_send.at[0, c], r_recv.at[slot, c],
+               jnp.clip(e + 1, 0, n_ep - 1), t).wait_recv()
+
+    inner = (e > 0) & (e < n_ep - 1)
+
+    def weights_to(d):
+        return remote(wts.at[e], wts.at[e], w_send.at[d - 1], w_recv.at[e], (e + d) % n_ep, t)
+
+    def weight_column(j):
+        held = wts[j]
+        mine = jnp.where(lax.broadcasted_iota(jnp.int32, held.shape, 0) == e, held, 0.0)
+        line = jnp.sum(mine, axis=0, keepdims=True)
+        shape = (rows, held.shape[1])
+        same = lax.broadcasted_iota(jnp.int32, shape, 0) == lax.broadcasted_iota(jnp.int32, shape, 1)
+        return jnp.sum(jnp.where(same, line, 0.0), axis=1, keepdims=True)
 
     loads["ei"].wait()
     loads["ng"].wait()
@@ -337,6 +364,15 @@
     lax.fori_loop(0, lane_rows // 16, norm_rows, 0)
     pl.semaphore_wait(barrier, len(greeted))
     spread(0)
+
+    place = lax.broadcasted_iota(jnp.int32, (wts.shape[1], rows), 0)
+    dense = jnp.zeros(place.shape, jnp.float32)
+    for k in range(ids.shape[0]):
+        dense += jnp.where(ids[k : k + 1, :] == place, rw[k : k + 1, :], 0.0)
+    wts[e] = jnp.zeros(wts.shape[1:], jnp.float32)
+    wts[e, :, 0:rows] = dense
+    for d in range(1, n_ep):
+        weights_to(d).start()
 
     loads["ig"].wait()
     loads["va"].wait()
@@ -417,22 +453,52 @@
             gather_forward(hid_slot(j), n_ep + j)
             gather_finish(hid_slot(j), n_ep + j)
             part = hid.shape[-1]
+
+            @pl.when(j != e)
+            def _():
+                remote(wts.at[e], wts.at[j], w_send.at[0], w_recv.at[j], j, t).wait_recv()
+
+            weight = weight_column(j)
             for c in range(chans // TILE):
                 at = slice(c * TILE, (c + 1) * TILE)
                 total = dot32(hid[j, 0], dw[0:part, at])
                 for lane in range(1, n_tp):
                     total += dot32(hid[j, lane], dw[lane * part : (lane + 1) * part, at])
-                res[j, :, at] = total.astype(jnp.bfloat16)
-
-            @pl.when(j != e)
+                res[j, :, at] = (weight * total).astype(jnp.bfloat16)
+
+            @pl.when((j != e) & ~inner)
             def _():
-                back(j).start()
+                for c in range(CHUNKS):
+                    hop(j, c).start()
 
         return 0
 
     lax.fori_loop(0, n_ep + 1, step, 0)
 
     gather_forward(shd_slot, shared_g)
+
+    for phase in range(2):
+        right = left_short if phase == 0 else ~left_short
+
+        def relay(d, _):
+            j = jnp.where(right, e + d, e - d)
+
+            @pl.when(inner & (j >= 0) & (j < n_ep))
+            def _():
+                def relay_piece(c, _):
+                    at = pl.ds(pl.multiple_of(c * piece, 16), piece)
+                    hop_arrives(j, c)
+                    total = res[j, at, :].astype(jnp.float32) + pin[j, at, :].astype(jnp.float32)
+                    res[j, at, :] = total.astype(jnp.bfloat16)
+                    hop(j, c).start()
+                    return 0
+
+                lax.fori_loop(0, CHUNKS, relay_piece, 0)
+
+            return 0
+
+        lax.fori_loop(1, n_ep, relay, 0)
+
     gather_forward(mixed_slot, mixed_g)
     gather_finish(shd_slot, shared_g)
     loads["sd"].wait()
@@ -449,9 +515,16 @@
 
     lax.fori_loop(0, chans // TILE, mixer_cols, 0)
 
-    for d in range(1, n_ep):
-        i = (e + d) % n_ep
-        remote(res.at[i], ret.at[i], r_send.at[i], r_recv.at[i], i, t).wait_recv()
+    for here, slot in ((e > 0, e), (e < n_ep - 1, n_ep)):
+
+        @pl.when(here)
+        def _():
+            for c in range(CHUNKS):
+                hop_arrives(slot, c)
+
+        @pl.when(~here)
+        def _():
+            pin[slot] = jnp.zeros(pin.shape[1:], pin.dtype)
 
     def combine_cols(c, _):
         at = pl.ds(pl.multiple_of(c * TILE, TILE), TILE)
@@ -459,11 +532,8 @@
         total = dot32(shd[0], sd[0:part, at])
         for lane in range(1, n_tp):
             total += dot32(shd[lane], sd[lane * part : (lane + 1) * part, at])
-        for d in range(n_ep):
-            i = (e + d) % n_ep
-            weight = jnp.sum(jnp.where(ids[...] == i, rw[...], 0.0), axis=1, keepdims=True)
-            found = res[e, :, at] if d == 0 else ret[i, :, at]
-            total += weight * found.astype(jnp.float32)
+        for found in (res[e, :, at], pin[e, :, at], pin[n_ep, :, at]):
+            total += found.astype(jnp.float32)
         exp_out[:, at] = total.astype(jnp.bfloat16)
         return 0
 
@@ -487,11 +557,14 @@
 
         @pl.when(j != e)
         def _():
-            back(j).wait_send()
+            for c in range(CHUNKS):
+                hop(j, c).wait_send()
 
         return 0
 
     lax.fori_loop(0, n_ep, drain, 0)
+    for d in range(1, n_ep):
+        weights_to(d).wait_send()
     gather_drain(shd_slot, shared_g)
     gather_drain(mixed_slot, mixed_g)
 
@@ -522,7 +595,8 @@
             pltpu.VMEM((rows, chans), bf),
             pltpu.VMEM((16, chans), bf),
             pltpu.VMEM((n_ep, rows, chans), bf),
-            pltpu.VMEM((n_ep, rows, chans), bf),
+            pltpu.VMEM((n_ep + 1, rows, chans), bf),
+            pltpu.VMEM((n_ep, -(-n_ep // 8) * 8, -(-rows // 128) * 128), f32),
             dma((len(big),)),
             dma((2, n_ep)),
             dma((n_ep,)),
@@ -530,6 +604,8 @@
             dma((sems, max(1, n_x - 1))),
             dma((sems, n_x)),
             dma((sems, n_x)),
+            dma((n_ep, CHUNKS)),
+            dma((n_ep + 1, CHUNKS)),
             dma((n_ep,)),
             dma((n_ep,)),
             dma((2,)),
@@ -537,7 +613,7 @@
         compiler_params=pltpu.CompilerParams(
             collective_id=0, has_side_effects=True, vmem_limit_bytes=60 * 1024 * 1024
         ),
-    )(ids, rw, *big)
+    )(ids.T, rw.T, *big)
 
 
 def local(*args):
@@ -548,6 +624,7 @@
         and lane_rows % 16 == 0
         and lane_rows * n_tp == args[0].shape[0]
         and chans % TILE == 0
+        and args[0].shape[0] % (16 * CHUNKS) == 0
         and args[9].shape[2] % 128 == 0
         and args[12].shape[1] % 128 == 0
     )

time: 96.6 us -> 91.8 us (0.950)
  the two profiles are of different devices: /device:TPU:24 before, /device:TPU:0 now
where the time goes in v2:
time: 91.8 us; the launch traced here: 91.6 us
  Pallas kernels  87.4 us (95%)
  local copies, waits for them, and re-layouts  3.53 us (4%)
    pallas_call x1, Pallas kernels, joined(): pl.pallas_call(functools.partial(kernel, n_ep, n_tp), out_shape=(out, out...  87.4 us
    unnamed x2, local copies, waits for them, and re-layouts  3.53 us

profile of v2, /device:TPU:0, one launch (start us, length us, event | category | flops | bytes accessed | tf_op | source)
XLA Modules:
  0.0 91.6 jit_solution(11743549878290760088)
XLA Ops:
  0.6 87.4 %shard_map.158 = (bf16[192,1024]{1,0:T(8,128)(2,1)}, bf16[192,1024]{1,0:T(8,128)(2,1)}) custom-call(s32[2,192]{1,0:T(2,128)} %bitcast.10, f32[2,192]{1,0:T(2,128)} %bitcast.11, bf16[192,1024]{1,0:T(8,128)(2,1)} %og_h.1, bf16[192,1024]{1,0:T(8,128)(2,1)} %ig_h.1, bf16[192,1024]{1,0:T(8,128)(2,1)} %va_h.1, f32[3,1024]{1,0:T(4,128)} %taps_h.1, ...), custom_call_target="tpu_custom_call" | custom-call | tf_op jit(solution)/shard_map/pallas_call | solution.py:584
  88.0 1.8 %copy.19 = bf16[192,1024]{1,0:T(8,128)(2,1)} copy(bf16[192,1024]{1,0:T(8,128)(2,1)} %get-tuple-element.4) | data formatting | bytes 786432
  89.8 1.8 %copy.20 = bf16[192,1024]{1,0:T(8,128)(2,1)} copy(bf16[192,1024]{1,0:T(8,128)(2,1)} %get-tuple-element.5) | data formatting | bytes 786432

commit v3 on v2

--- a/solution.py
+++ b/solution.py
@@ -10,6 +10,7 @@
 MESH = pl.DeviceIdType.MESH
 CORES = 2
 TILE = 256
+PIECE = 16
 CHUNKS = 4
 
 norm_floor = 0.5
@@ -270,10 +271,13 @@
             across(slot, g, d, from_x(d)).wait_send()
         across(slot, g, 0, t).wait_send()
 
-    shared_g, mixed_g = 2 * n_ep, 2 * n_ep + 1
-
-    def tok_slot(j):
-        return lambda lane: tok.at[j, lane]
+    pieces = lane_rows // PIECE
+    first_hidden = n_ep * pieces
+    shared_g = first_hidden + n_ep
+    mixed_g = shared_g + 1
+
+    def tok_slot(j, q):
+        return lambda lane: tok.at[j, lane, q]
 
     def hid_slot(j):
         return lambda lane: hid.at[j, lane]
@@ -292,13 +296,16 @@
         far = jnp.where(left_short, k, n_ep - 1 - k)
         return jnp.where(k <= 2 * nearest, near, far)
 
-    def z_right(j):
-        return remote(tok.at[j, t], tok.at[j, t], z_send.at[0, j], z_recv.at[j],
-                      jnp.minimum(e + 1, n_ep - 1), t)
-
-    def z_left(j):
-        return remote(tok.at[j, t], tok.at[j, t], z_send.at[1, j], z_recv.at[j],
-                      jnp.maximum(e - 1, 0), t)
+    def at_end(j):
+        return (j == 0) | (j == n_ep - 1)
+
+    def crosses(j):
+        return (j == e) | ~at_end(j)
+
+    def z_copy(side, d, j, q):
+        block = tok.at[j, from_x(d), q]
+        return remote(block, block, z_send.at[side, d, j, q], z_recv.at[d, j, q],
+                      jnp.clip(e + 1 - 2 * side, 0, n_ep - 1), t)
 
     def goes_right(j):
         return (j <= e) & (e < n_ep - 1)
@@ -306,22 +313,50 @@
     def goes_left(j):
         return (j >= e) & (e > 0)
 
-    def spread(k):
+    def z_onward(d, j, q):
+        @pl.when(goes_right(j))
+        def _():
+            z_copy(0, d, j, q).start()
+
+        @pl.when(goes_left(j))
+        def _():
+            z_copy(1, d, j, q).start()
+
+    def spread(k, q):
         j = block_at(k)
+        g = j * pieces + q
 
         @pl.when(k > 0)
         def _():
-            z_right(j).wait_recv()
-
-        @pl.when(goes_right(j))
-        def _():
-            z_right(j).start()
-
-        @pl.when(goes_left(j))
-        def _():
-            z_left(j).start()
-
-        gather_start(tok_slot(j), j)
+            z_copy(0, 0, j, q).wait_recv()
+
+        z_onward(0, j, q)
+
+        @pl.when(crosses(j))
+        def _():
+            for d in range(1, n_x):
+                cross(tok_slot(j, q), g, d, t).start()
+
+        across(tok_slot(j, q), g, 0, t).start()
+
+    def forward(k, q):
+        j = block_at(k)
+        g = j * pieces + q
+        for d in range(1, n_x):
+
+            @pl.when(crosses(j))
+            def _():
+                cross(tok_slot(j, q), g, d, from_x(d)).wait_recv()
+
+            @pl.when(~crosses(j))
+            def _():
+                z_copy(0, d, j, q).wait_recv()
+
+            @pl.when(at_end(j))
+            def _():
+                z_onward(d, j, q)
+
+            across(tok_slot(j, q), g, d, from_x(d)).start()
 
     piece = rows // CHUNKS
 
@@ -353,17 +388,18 @@
     loads["ng"].wait()
 
     def norm_rows(r, _):
-        at = pl.ds(pl.multiple_of(r * 16, 16), 16)
+        at = pl.ds(pl.multiple_of(r * PIECE, PIECE), PIECE)
         widened = ei[at, :].astype(jnp.float32)
         centred = widened - jnp.mean(widened, axis=-1, keepdims=True)
         spread_of = jnp.mean(centred * centred, axis=-1, keepdims=True)
         normed = centred * lax.rsqrt(spread_of + norm_floor) * ng[...]
-        tok[e, t, at, :] = normed.astype(jnp.bfloat16)
+        tok[e, t, r] = normed.astype(jnp.bfloat16)
         return 0
 
-    lax.fori_loop(0, lane_rows // 16, norm_rows, 0)
+    lax.fori_loop(0, pieces, norm_rows, 0)
     pl.semaphore_wait(barrier, len(greeted))
-    spread(0)
+    for q in range(pieces):
+        spread(0, q)
 
     place = lax.broadcasted_iota(jnp.int32, (wts.shape[1], rows), 0)
     dense = jnp.zeros(place.shape, jnp.float32)
@@ -423,35 +459,21 @@
         loads[name].wait()
 
     def step(s, _):
-        @pl.when(s + 1 < n_ep)
-        def _():
-            spread(s + 1)
-
-        @pl.when(s < n_ep)
-        def _():
-            j = block_at(s)
-            gather_forward(tok_slot(j), j)
-            gather_finish(tok_slot(j), j)
-            block = tok[j].reshape(rows, width)
-            hid[j, t] = silu_product(dot32(block, gw[...]), dot32(block, uw[...]))
-            gather_start(hid_slot(j), n_ep + j)
-
-        @pl.when(s == 0)
-        def _():
-            block = tok[e].reshape(rows, width)
-            shd[t] = silu_product(dot32(block, sg[...]), dot32(block, su[...]))
-            gather_start(shd_slot, shared_g)
-            loads["dw"].wait()
-
-        @pl.when(s == n_ep - 1)
-        def _():
-            gather_start(mixed_slot, mixed_g)
+        for q in range(pieces):
+
+            @pl.when(s + 1 < n_ep)
+            def _():
+                spread(s + 1, q)
+
+            @pl.when(s < n_ep)
+            def _():
+                forward(s, q)
 
         @pl.when(s >= 1)
         def _():
             j = block_at(s - 1)
-            gather_forward(hid_slot(j), n_ep + j)
-            gather_finish(hid_slot(j), n_ep + j)
+            gather_forward(hid_slot(j), first_hidden + j)
+            gather_finish(hid_slot(j), first_hidden + j)
             part = hid.shape[-1]
 
             @pl.when(j != e)
@@ -470,6 +492,26 @@
             def _():
                 for c in range(CHUNKS):
                     hop(j, c).start()
+
+        @pl.when(s < n_ep)
+        def _():
+            j = block_at(s)
+            for q in range(pieces):
+                gather_finish(tok_slot(j, q), j * pieces + q)
+            block = tok[j].reshape(rows, width)
+            hid[j, t] = silu_product(dot32(block, gw[...]), dot32(block, uw[...]))
+            gather_start(hid_slot(j), first_hidden + j)
+
+        @pl.when(s == 0)
+        def _():
+            block = tok[e].reshape(rows, width)
+            shd[t] = silu_product(dot32(block, sg[...]), dot32(block, su[...]))
+            gather_start(shd_slot, shared_g)
+            loads["dw"].wait()
+
+        @pl.when(s == n_ep - 1)
+        def _():
+            gather_start(mixed_slot, mixed_g)
 
         return 0
 
@@ -544,16 +586,32 @@
         halo_copy().wait_send()
 
     def drain(j, _):
-        @pl.when(goes_right(j))
-        def _():
-            z_right(j).wait_send()
-
-        @pl.when(goes_left(j))
-        def _():
-            z_left(j).wait_send()
-
-        gather_drain(tok_slot(j), j)
-        gather_drain(hid_slot(j), n_ep + j)
+        def drain_z(d, q):
+            @pl.when(goes_right(j))
+            def _():
+                z_copy(0, d, j, q).wait_send()
+
+            @pl.when(goes_left(j))
+            def _():
+                z_copy(1, d, j, q).wait_send()
+
+        for q in range(pieces):
+            g = j * pieces + q
+            drain_z(0, q)
+            across(tok_slot(j, q), g, 0, t).wait_send()
+            for d in range(1, n_x):
+
+                @pl.when(crosses(j))
+                def _():
+                    cross(tok_slot(j, q), g, d, t).wait_send()
+
+                @pl.when(at_end(j))
+                def _():
+                    drain_z(d, q)
+
+                across(tok_slot(j, q), g, d, from_x(d)).wait_send()
+
+        gather_drain(hid_slot(j), first_hidden + j)
 
         @pl.when(j != e)
         def _():
@@ -576,7 +634,8 @@
     rows, chans = og.shape
     lane_rows, width = ei.shape
     n_x = n_tp // CORES
-    sems = 2 * n_ep + 2
+    pieces = lane_rows // PIECE
+    sems = n_ep * pieces + n_ep + 2
     big = (og, ig, va, taps, mw, ei, ng, gw, uw, dw, sg, su, sd)
     out = jax.ShapeDtypeStruct((rows, chans), bf)
     vmem = pl.BlockSpec(memory_space=pltpu.VMEM)
@@ -588,7 +647,7 @@
         out_specs=(vmem, vmem),
         scratch_shapes=[pltpu.VMEM(a.shape, a.dtype) for a in big]
         + [
-            pltpu.VMEM((n_ep, n_tp, lane_rows, width), bf),
+            pltpu.VMEM((n_ep, n_tp, pieces, PIECE, width), bf),
             pltpu.VMEM((n_ep, n_tp, rows, gw.shape[-1]), bf),
             pltpu.VMEM((n_tp, rows, sg.shape[-1]), bf),
             pltpu.VMEM((n_tp, rows, chans), bf),
@@ -598,8 +657,8 @@
             pltpu.VMEM((n_ep + 1, rows, chans), bf),
             pltpu.VMEM((n_ep, -(-n_ep // 8) * 8, -(-rows // 128) * 128), f32),
             dma((len(big),)),
-            dma((2, n_ep)),
-            dma((n_ep,)),
+            dma((2, n_x, n_ep, pieces)),
+            dma((n_x, n_ep, pieces)),
             dma((sems, max(1, n_x - 1))),
             dma((sems, max(1, n_x - 1))),
             dma((sems, n_x)),
@@ -621,7 +680,7 @@
     chans, lane_rows = args[0].shape[1], args[5].shape[0]
     aligned = (
         n_tp % CORES == 0
-        and lane_rows % 16 == 0
+        and lane_rows % PIECE == 0
         and lane_rows * n_tp == args[0].shape[0]
         and chans % TILE == 0
         and args[0].shape[0] % (16 * CHUNKS) == 0

time: 91.8 us -> 88.1 us (0.960)
  Pallas kernels: 87.4 us -> 83.7 us
    pallas_call x1, Pallas kernels: 87.4 us -> 83.7 us  [joined(): pl.pallas_call(functools.partial(kernel, n_ep, n_tp), out_shape=(out, out...]
where the time goes in v3:
time: 88.1 us; the launch traced here: 87.8 us
  Pallas kernels  83.7 us (95%)
  local copies, waits for them, and re-layouts  3.53 us (4%)
    pallas_call x1, Pallas kernels, joined(): pl.pallas_call(functools.partial(kernel, n_ep, n_tp), out_shape=(out, out...  83.7 us
    unnamed x2, local copies, waits for them, and re-layouts  3.53 us

profile of v3, /device:TPU:0, one launch (start us, length us, event | category | flops | bytes accessed | tf_op | source)
XLA Modules:
  0.0 87.8 jit_solution(6721552884480526108)
XLA Ops:
  0.6 83.7 %shard_map.158 = (bf16[192,1024]{1,0:T(8,128)(2,1)}, bf16[192,1024]{1,0:T(8,128)(2,1)}) custom-call(s32[2,192]{1,0:T(2,128)} %bitcast.10, f32[2,192]{1,0:T(2,128)} %bitcast.11, bf16[192,1024]{1,0:T(8,128)(2,1)} %og_h.1, bf16[192,1024]{1,0:T(8,128)(2,1)} %ig_h.1, bf16[192,1024]{1,0:T(8,128)(2,1)} %va_h.1, f32[3,1024]{1,0:T(4,128)} %taps_h.1, ...), custom_call_target="tpu_custom_call" | custom-call | tf_op jit(solution)/shard_map/pallas_call | solution.py:643
  84.3 1.8 %copy.19 = bf16[192,1024]{1,0:T(8,128)(2,1)} copy(bf16[192,1024]{1,0:T(8,128)(2,1)} %get-tuple-element.4) | data formatting | bytes 786432
  86.1 1.8 %copy.20 = bf16[192,1024]{1,0:T(8,128)(2,1)} copy(bf16[192,1024]{1,0:T(8,128)(2,1)} %get-tuple-element.5) | data formatting | bytes 786432

commit v4 on v3

--- a/solution.py
+++ b/solution.py
@@ -458,60 +458,73 @@
     for name in ("gw", "uw", "sg", "su"):
         loads[name].wait()
 
-    def step(s, _):
+    def leave(k, _):
+        j = block_at(k)
+        gather_forward(hid_slot(j), first_hidden + j)
+        gather_finish(hid_slot(j), first_hidden + j)
+        part = hid.shape[-1]
+
+        @pl.when(j != e)
+        def _():
+            remote(wts.at[e], wts.at[j], w_send.at[0], w_recv.at[j], j, t).wait_recv()
+
+        weight = weight_column(j)
+        for c in range(chans // TILE):
+            at = slice(c * TILE, (c + 1) * TILE)
+            total = dot32(hid[j, 0], dw[0:part, at])
+            for lane in range(1, n_tp):
+                total += dot32(hid[j, lane], dw[lane * part : (lane + 1) * part, at])
+            res[j, :, at] = (weight * total).astype(jnp.bfloat16)
+
+        @pl.when((j != e) & ~inner)
+        def _():
+            for c in range(CHUNKS):
+                hop(j, c).start()
+        return 0
+
+    def meet(k):
+        j = block_at(k)
         for q in range(pieces):
-
-            @pl.when(s + 1 < n_ep)
-            def _():
-                spread(s + 1, q)
-
-            @pl.when(s < n_ep)
-            def _():
-                forward(s, q)
-
-        @pl.when(s >= 1)
-        def _():
-            j = block_at(s - 1)
-            gather_forward(hid_slot(j), first_hidden + j)
-            gather_finish(hid_slot(j), first_hidden + j)
-            part = hid.shape[-1]
-
-            @pl.when(j != e)
-            def _():
-                remote(wts.at[e], wts.at[j], w_send.at[0], w_recv.at[j], j, t).wait_recv()
-
-            weight = weight_column(j)
-            for c in range(chans // TILE):
-                at = slice(c * TILE, (c + 1) * TILE)
-                total = dot32(hid[j, 0], dw[0:part, at])
-                for lane in range(1, n_tp):
-                    total += dot32(hid[j, lane], dw[lane * part : (lane + 1) * part, at])
-                res[j, :, at] = (weight * total).astype(jnp.bfloat16)
-
-            @pl.when((j != e) & ~inner)
-            def _():
-                for c in range(CHUNKS):
-                    hop(j, c).start()
-
-        @pl.when(s < n_ep)
-        def _():
-            j = block_at(s)
-            for q in range(pieces):
-                gather_finish(tok_slot(j, q), j * pieces + q)
-            block = tok[j].reshape(rows, width)
-            hid[j, t] = silu_product(dot32(block, gw[...]), dot32(block, uw[...]))
-            gather_start(hid_slot(j), first_hidden + j)
-
-        @pl.when(s == 0)
+            gather_finish(tok_slot(j, q), j * pieces + q)
+        block = tok[j].reshape(rows, width)
+        hid[j, t] = silu_product(dot32(block, gw[...]), dot32(block, uw[...]))
+        gather_start(hid_slot(j), first_hidden + j)
+
+        @pl.when(k == 0)
         def _():
             block = tok[e].reshape(rows, width)
             shd[t] = silu_product(dot32(block, sg[...]), dot32(block, su[...]))
             gather_start(shd_slot, shared_g)
             loads["dw"].wait()
 
-        @pl.when(s == n_ep - 1)
+        @pl.when(k == n_ep - 1)
         def _():
             gather_start(mixed_slot, mixed_g)
+
+    def step(s, _):
+        for q in range(pieces):
+
+            @pl.when(s + 1 < n_ep)
+            def _():
+                spread(s + 1, q)
+
+            @pl.when(s < n_ep)
+            def _():
+                forward(s, q)
+
+        @pl.when(~inner)
+        def _():
+            lax.fori_loop(jnp.maximum(s - 1, 0), s, leave, 0)
+
+        k = jnp.where(inner, s - 1, s)
+
+        @pl.when((k >= 0) & (k < n_ep))
+        def _():
+            meet(k)
+
+        @pl.when(inner & (s == n_ep))
+        def _():
+            lax.fori_loop(0, n_ep, leave, 0)
 
         return 0
 

time: 88.1 us -> 85.7 us (0.973)
  Pallas kernels: 83.7 us -> 81.3 us
    pallas_call x1, Pallas kernels: 83.7 us -> 81.3 us  [joined(): pl.pallas_call(functools.partial(kernel, n_ep, n_tp), out_shape=(out, out...]
where the time goes in v4:
time: 85.7 us; the launch traced here: 85.4 us
  Pallas kernels  81.3 us (95%)
  local copies, waits for them, and re-layouts  3.53 us (4%)
    pallas_call x1, Pallas kernels, joined(): pl.pallas_call(functools.partial(kernel, n_ep, n_tp), out_shape=(out, out...  81.3 us
    unnamed x2, local copies, waits for them, and re-layouts  3.53 us

profile of v4, /device:TPU:0, one launch (start us, length us, event | category | flops | bytes accessed | tf_op | source)
XLA Modules:
  0.0 85.4 jit_solution(5186803444216924334)
XLA Ops:
  0.6 81.3 %shard_map.158 = (bf16[192,1024]{1,0:T(8,128)(2,1)}, bf16[192,1024]{1,0:T(8,128)(2,1)}) custom-call(s32[2,192]{1,0:T(2,128)} %bitcast.10, f32[2,192]{1,0:T(2,128)} %bitcast.11, bf16[192,1024]{1,0:T(8,128)(2,1)} %og_h.1, bf16[192,1024]{1,0:T(8,128)(2,1)} %ig_h.1, bf16[192,1024]{1,0:T(8,128)(2,1)} %va_h.1, f32[3,1024]{1,0:T(4,128)} %taps_h.1, ...), custom_call_target="tpu_custom_call" | custom-call | tf_op jit(solution)/shard_map/pallas_call | solution.py:656
  81.9 1.8 %copy.19 = bf16[192,1024]{1,0:T(8,128)(2,1)} copy(bf16[192,1024]{1,0:T(8,128)(2,1)} %get-tuple-element.4) | data formatting | bytes 786432
  83.7 1.8 %copy.20 = bf16[192,1024]{1,0:T(8,128)(2,1)} copy(bf16[192,1024]{1,0:T(8,128)(2,1)} %get-tuple-element.5) | data formatting | bytes 786432
